TPU v7x, 512 devices: a whole 4x8x8 slice. The times are simulated.
512 devices in a mesh: ep: 32 (over z, x), tp: 16 (over y, core).
Axes of the slice: x: 4, y: 8, z: 8, core: 2. Of those that a mesh axis runs over, the one named last changes fastest.
Arguments:
- mix_input: bfloat16 [16384, 2048], P('ep', 'tp'), may hold values from -6 to 6
- mix_weight: bfloat16 [2048, 4096], P(None, 'tp'), may hold values from -0.125 to 0.125
- expert_input: bfloat16 [4096, 4096], P('ep', 'tp'), may hold values from -4500 to 4500
- expert_index: int32 [4096, 2], P('ep'), may hold values from 0 to 31, as said below
- route_share: float32 [4096, 2], P('ep'), may hold values from 0.1 to 1
- norm_gain: float32 [4096], replicated, may hold values from 0.1 to 1.9
- gate_weight: bfloat16 [32, 4096, 2048], P('ep', None, 'tp'), may hold values from -0.09375 to 0.09375
- up_weight: bfloat16 [32, 4096, 2048], P('ep', None, 'tp'), may hold values from -0.09375 to 0.09375
- down_weight: bfloat16 [32, 2048, 4096], P('ep', None, 'tp'), may hold values from -0.125 to 0.125
Outputs:
- mixed_rows: bfloat16 [16384, 4096], P('ep', 'tp')
- expert_rows: bfloat16 [4096, 4096], P('ep', 'tp')
Inputs may be any that keep to these rules, and one draw needn't show every extreme that they name: `expert_index`: each row names 2 different experts. Within each aligned block of 128 rows (the rows of one index of ep) no expert is named by more than 16 rows, and one expert, the same in every block, is named by exactly 16 rows.
All inputs are finite; a program needn't handle non-finite values.
Results may differ from a plain program's by a relative error of at most 0.007.
Values may be sent and summed in bfloat16 or wider, within the bound.
No kernel may reach another device: no remote copies, remote signals or barrier semaphores. Data moves between devices by JAX's collectives and lax.ppermute only.
A program may use at most 64 MiB of HBM per device.

v0:
```python
import jax
import jax.numpy as jnp
from jax import lax
from jax.sharding import PartitionSpec as P

POOL = 2048
TOP = 2
window_reach = 15
norm_eps = 1e-06


def passed_along(value, axis, by):
    size = lax.axis_size(axis)
    pairs = [(i, i + by) for i in range(size) if 0 <= i + by < size]
    return lax.ppermute(value, axis, pairs)


def laid_out(parts, dim):
    lengths = list(parts.shape[1:])
    lengths[dim] *= parts.shape[0]
    return jnp.moveaxis(parts, 0, dim).reshape(lengths)


def copy_for_each(value, axis):
    size = lax.axis_size(axis)
    return lax.all_to_all(
        jnp.broadcast_to(value[None], (size, *value.shape)), axis, 0, 0, tiled=True
    )


def gathered_copies(value, axis, dim):
    return laid_out(copy_for_each(value, axis), dim)


def pool_minus_self(extended, first_pos, group_size, channel_base):
    length = extended.shape[0] - window_reach
    channels = extended.shape[1]
    channel = channel_base + jnp.arange(channels, dtype=jnp.int32)
    window = jnp.power(2, channel // group_size + 1).astype(jnp.int32)
    running = jnp.zeros((length, channels), jnp.float32)
    for lag_count in range(window_reach + 1):
        shifted = extended[window_reach - lag_count : window_reach - lag_count + length]
        running = running + jnp.where(lag_count < window[None, :], shifted, 0.0)
    position = first_pos + jnp.arange(length, dtype=jnp.int32)
    counts = jnp.minimum(position[:, None] + 1, window[None, :]).astype(jnp.float32)
    return (running / counts - extended[window_reach:]).astype(jnp.bfloat16)


def slot_targets(indices, experts, capacity):
    flattened = indices.reshape(-1)
    one_hot = (flattened[:, None] == jnp.arange(experts, dtype=jnp.int32)[None, :]).astype(
        jnp.int32
    )
    earlier = jnp.cumsum(one_hot, axis=0) - one_hot
    return flattened * capacity + jnp.sum(earlier * one_hot, axis=1)


def shards(
    mix_input,
    mix_weight,
    expert_input,
    expert_index,
    route_share,
    norm_gain,
    gate_weight,
    up_weight,
    down_weight,
):
    tokens_mix, channels = mix_input.shape
    trailing = mix_input[tokens_mix - window_reach :]
    previous = passed_along(trailing, "ep", 1)
    extended = jnp.concatenate([previous, mix_input], axis=0).astype(jnp.float32)
    pooled = pool_minus_self(
        extended, lax.axis_index("ep") * tokens_mix, POOL // 4, lax.axis_index("tp") * channels
    )
    mixed_rows = jnp.dot(
        lax.all_gather(pooled, "tp", axis=1, tiled=True),
        mix_weight,
        preferred_element_type=jnp.float32,
    ).astype(jnp.bfloat16)
    tokens_exp = expert_input.shape[0]
    local_experts = gate_weight.shape[0]
    experts = local_experts * lax.axis_size("ep")
    capacity = 2 * tokens_exp * TOP // experts
    model_width = norm_gain.shape[0]
    targets = slot_targets(expert_index, experts, capacity)
    sources = jnp.repeat(jnp.arange(tokens_exp, dtype=jnp.int32), TOP)
    table = jnp.full((experts * capacity,), tokens_exp, jnp.int32).at[targets].set(sources)
    feature_block = expert_input.shape[1]
    padded = jnp.concatenate([expert_input, jnp.zeros((1, feature_block), jnp.bfloat16)], axis=0)
    outgoing = padded[table].reshape(experts, capacity, feature_block)
    arrived = lax.all_to_all(outgoing, "ep", split_axis=0, concat_axis=1, tiled=True)
    portion = lax.all_gather(arrived, "tp", axis=2, tiled=True)
    scaled = (portion.astype(jnp.float32) * norm_gain).astype(jnp.bfloat16)
    gate_acts = jnp.einsum("erd,edh->erh", scaled, gate_weight, preferred_element_type=jnp.float32)
    up_acts = jnp.einsum("erd,edh->erh", scaled, up_weight, preferred_element_type=jnp.float32)
    squares = jnp.sum(jnp.square(portion.astype(jnp.float32)), axis=2)
    inverse = lax.rsqrt(squares / model_width + norm_eps)[:, :, None]
    hidden = (jax.nn.silu(gate_acts * inverse) * (up_acts * inverse)).astype(jnp.bfloat16)
    produced = jnp.einsum(
        "erh,ehc->erc",
        gathered_copies(hidden, "tp", 2),
        down_weight,
        preferred_element_type=jnp.float32,
    ).astype(jnp.bfloat16)
    returned = lax.all_to_all(produced, "ep", split_axis=1, concat_axis=0, tiled=True)
    returned = returned.reshape(experts * capacity, returned.shape[2])
    picked = returned[targets].astype(jnp.float32).reshape(tokens_exp, TOP, returned.shape[1])
    shares = route_share / jnp.sum(route_share, axis=1, keepdims=True)
    expert_rows = jnp.sum(picked * shares[:, :, None], axis=1).astype(jnp.bfloat16)
    return (mixed_rows, expert_rows)


def solution(mesh):
    placed = (
        P("ep", "tp"),
        P(None, "tp"),
        P("ep", "tp"),
        P("ep", None),
        P("ep", None),
        P(),
        P("ep", None, "tp"),
        P("ep", None, "tp"),
        P("ep", None, "tp"),
    )
    return jax.shard_map(
        shards,
        mesh=mesh,
        in_specs=placed,
        out_specs=(P("ep", "tp"), P("ep", "tp")),
        check_vma=False,
    )
```

profile of v0, /device:TPU:24, one launch (start us, length us, event | category | flops | bytes accessed | tf_op | source)
XLA Modules:
  0.0 192.1 jit_solution(15322384750593228259)
XLA Ops:
  7.2 0.0 copy-start
  7.2 0.0 copy-start.6
  7.2 0.0 copy-start.4
  7.2 0.0 all-gather.5.cloned.1.call-start
  7.2 0.8 broadcast_multiply_fusion
  8.1 0.8 copy.27
  8.8 0.1 eq.29
  9.0 0.1 eq.25
  9.1 0.1 copy.26
  9.2 0.1 mul.314
  9.4 0.6 reduce-window.6
  10.0 0.2 slice_reduce_fusion
  10.2 0.1 reshape.270
  10.4 0.1 fusion.43
  10.5 1.4 scatter_custom_fusion
  11.9 0.8 concatenate.7
  12.8 1.9 %gather_fusion = bf16[512,256]{1,0:T(8,128)(2,1)S(1)} fusion(bf16[129,256]{1,0:T(8,128)(2,1)S(1)} %concatenate.7, s32[1024]{0:T(1024)S(1)} %pad_clamp_fusion.1), kind=kCustom, calls=%fused_computation | custom fusion | bytes 526336 | tf_op jit(solution)/shard_map/gather | solution.py:91
  14.7 25.9 %all_to_all.26 = bf16[32,16,256]{2,1,0:T(8,128)(2,1)} all-to-all(bf16[32,16,256]{2,1,0:T(8,128)(2,1)S(1)} %bitcast.67), channel_id=1, replica_groups=mesh['ep'=32,'tp'=16] {'ep'}, dimensions={0} | all-to-all | bytes 524288 | tf_op jit(solution)/shard_map/all_to_all | solution.py:92
  40.6 0.0 all-gather.5.cloned.1.call-update
  40.6 0.7 slice.58
  41.3 2.1 %collective-permute-start = (bf16[15,128]{1,0:T(8,128)(2,1)S(1)}, bf16[15,128]{1,0:T(8,128)(2,1)S(1)}, u32[]{:S(2)}, u32[]{:S(2)}) collective-permute-start(bf16[15,128]{1,0:T(8,128)(2,1)S(1)} %slice.58), channel_id=1, source_target_pairs={{0,16},{16,32},{32,48},{48,64},{64,80},{80,96},{96,112},{112,128},... | collective-permute-start | bytes 11528 | tf_op jit(solution)/shard_map/ppermute | solution.py:15
  43.6 42.6 %all-gather.5.cloned.1.call-done = bf16[1,512,4096]{2,1,0:T(8,128)(2,1)} async-done(((bf16[1,512,256]{2,1,0:T(8,128)(2,1)}), bf16[1,512,4096]{2,1,0:T(8,128)(2,1)}) %all-gather.5.cloned.1.call-update) | async-done | bytes 4194320 | tf_op jit(solution)/shard_map/all_gather | solution.py:93
  86.2 0.0 copy-start.1
  86.2 3.2 %fusion.1 = f32[512]{0:T(512)S(1)} fusion(bf16[1,512,4096]{2,1,0:T(8,128)(2,1)} %all-gather.5.cloned.1.call-done), kind=kLoop, calls=%fused_computation.6 | loop fusion | flops 6290944 | bytes 4196352 | tf_op jit(solution)/shard_map/reduce_sum | solution.py:97
  89.4 0.0 copy-start.5
  89.4 0.0 copy-done.6
  89.4 0.0 copy-done.4
  89.4 0.2 copy-done.1
  89.6 1.3 fusion.8
  90.9 0.0 copy-done.5
  90.9 1.3 fusion.17
  92.2 0.0 copy-start.2
  92.2 0.1 copy.30
  92.3 1.5 broadcast_in_dim.167
  93.8 0.0 copy-start.3
  93.8 6.5 %all-to-all-start.1 = ((bf16[16,1,512,128]{2,3,1,0:T(8,128)(2,1)}), bf16[16,1,512,128]{2,3,1,0:T(8,128)(2,1)S(1)}, u32[]{:S(2)}, u32[]{:S(2)}) async-start(bf16[16,1,512,128]{2,3,1,0:T(8,128)(2,1)} %broadcast_in_dim.167), calls=%async_computation.1 | async-start | bytes 4194304 | tf_op jit(solution)/shard_map/all_to_all | solution.py:26
  100.3 0.0 all-gather.3.cloned.1.call-start
  100.4 0.0 collective-permute-done
  100.4 0.0 copy-done.2
  100.4 1.2 fusion.40
  101.7 0.0 all-gather.3.cloned.1.call-update
  101.7 0.0 copy-done.3
  101.7 52.9 %all-to-all-done.1 = bf16[16,1,512,128]{2,3,1,0:T(8,128)(2,1)S(1)} async-done(((bf16[16,1,512,128]{2,3,1,0:T(8,128)(2,1)}), bf16[16,1,512,128]{2,3,1,0:T(8,128)(2,1)S(1)}, u32[]{:S(2)}, u32[]{:S(2)}) %all-to-all-start.1) | async-done | bytes 2097184 | tf_op jit(solution)/shard_map/all_to_all | solution.py:26
  154.6 0.0 copy-done
  154.6 0.8 fusion.7
  155.4 0.4 copy.40
  155.8 0.5 broadcast.1945
  156.3 2.3 %reduce.3 = bf16[512,256]{1,0:T(8,128)(2,1)S(1)} reduce(bf16[512,1,256]{2,1,0:T(2,128)(2,1)S(1)} %bitcast.65, bf16[]{:T(256)} %broadcast.1945), dimensions={1}, to_apply=%bitcast.60.reduce_sub_computation | reduce | bytes 524290
  158.6 0.8 reshape.278
  159.4 10.0 %all-to-all-start.2 = ((bf16[32,2,2048]{2,1,0:T(2,128)(2,1)}), bf16[32,2,2048]{2,1,0:T(2,128)(2,1)S(1)}, u32[]{:S(2)}, u32[]{:S(2)}) async-start(bf16[32,2,2048]{2,1,0:T(2,128)(2,1)} %reshape.278), calls=%async_computation.2 | async-start | bytes 524288 | tf_op jit(solution)/shard_map/all_to_all | solution.py:106
  169.4 0.1 copy.33
  169.5 0.0 all-gather.3.cloned.1.call-done
  169.5 3.3 %convolution_convert_fusion.1 = bf16[512,256]{1,0:T(8,128)(2,1)} fusion(bf16[512,2048]{1,0:T(8,128)(2,1)} %all-gather.3.cloned.1.call-done, bf16[2048,256]{1,0:T(8,128)(2,1)} %param.10), kind=kOutput, calls=%fused_computation.11 | convolution fusion | flops 537001984 | bytes 3407872 | tf_op jit(solution)/shard_map/dot_general | solution.py:76
  172.8 9.8 %all-to-all-done.2 = bf16[32,2,2048]{2,1,0:T(2,128)(2,1)S(1)} async-done(((bf16[32,2,2048]{2,1,0:T(2,128)(2,1)}), bf16[32,2,2048]{2,1,0:T(2,128)(2,1)S(1)}, u32[]{:S(2)}, u32[]{:S(2)}) %all-to-all-start.2) | async-done | bytes 262176 | tf_op jit(solution)/shard_map/all_to_all | solution.py:106
  182.6 0.3 reshape.279
  182.9 1.2 gather_fusion.1
  184.1 0.1 reshape.249
  184.2 1.0 multiply_reduce_fusion
  (23 shorter events, 0.4 us)
Async XLA Ops:
  7.2 147.4 %copy-start = (bf16[1,2048,256]{2,1,0:T(8,128)(2,1)S(1)}, bf16[1,2048,256]{2,1,0:T(8,128)(2,1)}, u32[]{:S(2)}) copy-start(bf16[1,2048,256]{2,1,0:T(8,128)(2,1)} %param.17) | copy-start | bytes 3145732
  7.2 82.2 %copy-start.6 = (f32[4096]{0:T(1024)S(1)}, f32[4096]{0:T(1024)}, u32[]{:S(2)}) copy-start(f32[4096]{0:T(1024)} %param.14) | copy-start | bytes 49156
  7.2 82.2 %copy-start.4 = (bf16[1,4096,128]{2,1,0:T(8,128)(2,1)S(1)}, bf16[1,4096,128]{2,1,0:T(8,128)(2,1)}, u32[]{:S(2)}) copy-start(bf16[1,4096,128]{2,1,0:T(8,128)(2,1)} %param.15) | copy-start | bytes 3145732
  7.2 79.0 %all-gather.5.cloned.1.call-start = ((), (), s32[]{:S(2)}) async-start(), calls=%async_computation.4 | async-start | bytes 4456448 | tf_op jit(solution)/shard_map/all_gather | solution.py:93
  41.3 59.1 %collective-permute-start = (bf16[15,128]{1,0:T(8,128)(2,1)S(1)}, bf16[15,128]{1,0:T(8,128)(2,1)S(1)}, u32[]{:S(2)}, u32[]{:S(2)}) collective-permute-start(bf16[15,128]{1,0:T(8,128)(2,1)S(1)} %slice.58), channel_id=1, source_target_pairs={{0,16},{16,32},{32,48},{48,64},{64,80},{80,96},{96,112},{112,128},... | collective-permute-start | bytes 11528 | tf_op jit(solution)/shard_map/ppermute | solution.py:15
  86.2 3.4 %copy-start.1 = (bf16[1,512,4096]{2,1,0:T(8,128)(2,1)S(1)}, bf16[1,512,4096]{2,1,0:T(8,128)(2,1)}, u32[]{:S(2)}) copy-start(bf16[1,512,4096]{2,1,0:T(8,128)(2,1)} %all-gather.5.cloned.1.call-done) | copy-start | bytes 12582916
  89.4 1.5 copy-start.5
  92.2 8.2 %copy-start.2 = (bf16[512,128]{1,0:T(8,128)(2,1)S(1)}, bf16[512,128]{1,0:T(8,128)(2,1)}, u32[]{:S(2)}) copy-start(bf16[512,128]{1,0:T(8,128)(2,1)} %param.9) | copy-start | bytes 393220
  93.8 7.9 %copy-start.3 = (f32[128,2]{0,1:T(2,128)S(1)}, f32[128,2]{0,1:T(2,128)}, u32[]{:S(2)}) copy-start(f32[128,2]{0,1:T(2,128)} %param.13) | copy-start | bytes 3076
  93.8 60.8 %all-to-all-start.1 = ((bf16[16,1,512,128]{2,3,1,0:T(8,128)(2,1)}), bf16[16,1,512,128]{2,3,1,0:T(8,128)(2,1)S(1)}, u32[]{:S(2)}, u32[]{:S(2)}) async-start(bf16[16,1,512,128]{2,3,1,0:T(8,128)(2,1)} %broadcast_in_dim.167), calls=%async_computation.1 | async-start | bytes 4194304 | tf_op jit(solution)/shard_map/all_to_all | solution.py:26
  100.3 69.2 %all-gather.3.cloned.1.call-start = ((), (), s32[]{:S(2)}) async-start(), calls=%async_computation.3 | async-start | bytes 2228224 | tf_op jit(solution)/shard_map/all_gather | solution.py:77
  159.4 23.2 %all-to-all-start.2 = ((bf16[32,2,2048]{2,1,0:T(2,128)(2,1)}), bf16[32,2,2048]{2,1,0:T(2,128)(2,1)S(1)}, u32[]{:S(2)}, u32[]{:S(2)}) async-start(bf16[32,2,2048]{2,1,0:T(2,128)(2,1)} %reshape.278), calls=%async_computation.2 | async-start | bytes 524288 | tf_op jit(solution)/shard_map/all_to_all | solution.py:106
Sparse Core Ops, SparseCore 0:
  40.7 45.3 all-gather.4
  103.7 61.7 all-gather.2
where the time goes:
time: 192 us
  waiting for transfers between devices  105 us (55%)
  blocking collectives  25.9 us (13%)
  starting transfers between devices  18.6 us (10%)
  between operations  14.3 us (7%)
  local copies, waits for them, and re-layouts  11.8 us (6%)
  other arithmetic  9.6 us (5%)
  matrix products  6.54 us (3%)
    all_to_all x1, waiting for transfers between devices, copy_for_each(): lax.all_to_all(jnp.broadcast_to(value[None], (size, *value.shape)), axis,...  52.9 us
    all_gather x1, waiting for transfers between devices, shards(): portion = lax.all_gather(arrived, 'tp', axis=2, tiled=True)  42.6 us
    all_to_all x1, blocking collectives, shards(): lax.all_to_all(outgoing, 'ep', split_axis=0, concat_axis=1, tiled=True)  25.9 us
    all_to_all x1, starting transfers between devices, shards(): lax.all_to_all(produced, 'ep', split_axis=1, concat_axis=0, tiled=True)  9.99 us
    all_to_all x1, waiting for transfers between devices, shards(): lax.all_to_all(produced, 'ep', split_axis=1, concat_axis=0, tiled=True)  9.79 us
    all_to_all x1, starting transfers between devices, copy_for_each(): lax.all_to_all(jnp.broadcast_to(value[None], (size, *value.shape)), axis,...  6.49 us
  transfers between devices with their start and end apart: 5, of which 3 were waited for; matrix products, arithmetic and copies ran while one was open for 9% of the time, Pallas kernels for 0%

commit v1 on v0

--- a/solution.py
+++ b/solution.py
@@ -66,6 +66,38 @@
     up_weight,
     down_weight,
 ):
+
+    def extend_heaps(d_out, local_array):
+        p_next, base_arr, t_next = (
+            lax.axis_size("tp"),
+            lax.axis_index("tp"),
+            local_array.shape[d_out],
+        )
+        last = range(p_next)
+        q_next = map(lambda u: (u, (u + 1) % p_next), last)
+        steps_seen = list(q_next)
+        oldest = range(p_next)
+        v_now = map(lambda u: (u, (u - 1) % p_next), oldest)
+        gallery = list(v_now)
+        t1 = jnp.zeros(
+            (*local_array.shape[:d_out], p_next * t_next, *local_array.shape[d_out + 1 :]),
+            local_array.dtype,
+        )
+        t1 = lax.dynamic_update_slice_in_dim(t1, local_array, base_arr * t_next, axis=d_out)
+        block_now = built = local_array
+        a_next = p_next // 2
+        for h in range(1, a_next + 1):
+            block_now = lax.ppermute(block_now, "tp", steps_seen)
+            t1 = lax.dynamic_update_slice_in_dim(
+                t1, block_now, (base_arr - h) % p_next * t_next, axis=d_out
+            )
+            if h < p_next - a_next:
+                built = lax.ppermute(built, "tp", gallery)
+                t1 = lax.dynamic_update_slice_in_dim(
+                    t1, built, (base_arr + h) % p_next * t_next, axis=d_out
+                )
+        return t1
+
     tokens_mix, channels = mix_input.shape
     trailing = mix_input[tokens_mix - window_reach :]
     previous = passed_along(trailing, "ep", 1)
@@ -90,7 +122,7 @@
     padded = jnp.concatenate([expert_input, jnp.zeros((1, feature_block), jnp.bfloat16)], axis=0)
     outgoing = padded[table].reshape(experts, capacity, feature_block)
     arrived = lax.all_to_all(outgoing, "ep", split_axis=0, concat_axis=1, tiled=True)
-    portion = lax.all_gather(arrived, "tp", axis=2, tiled=True)
+    portion = extend_heaps(2, arrived)
     scaled = (portion.astype(jnp.float32) * norm_gain).astype(jnp.bfloat16)
     gate_acts = jnp.einsum("erd,edh->erh", scaled, gate_weight, preferred_element_type=jnp.float32)
     up_acts = jnp.einsum("erd,edh->erh", scaled, up_weight, preferred_element_type=jnp.float32)

time: 192 us -> 196 us (1.021)
  starting transfers between devices: 18.6 us -> 56.5 us
  waiting for transfers between devices: 105 us -> 72.7 us
  other arithmetic: 9.6 us -> 7.06 us
    all_gather x1 -> x0, waiting for transfers between devices: 42.6 us -> none  [shards(): portion = lax.all_gather(arrived, 'tp', axis=2, tiled=True)]
    ppermute x0 -> x15, starting transfers between devices: none -> 34.9 us  [the longest x8 25.9 us: extend_heaps(): block_now = lax.ppermute(block_now, 'tp', steps_seen)]
    ppermute x0 -> x15, waiting for transfers between devices: none -> 10.2 us  [the longest x8 6.49 us: extend_heaps(): block_now = lax.ppermute(block_now, 'tp', steps_seen)]
    all_to_all x1, starting transfers between devices: 6.49 us -> 14.1 us  [copy_for_each(): lax.all_to_all(jnp.broadcast_to(value[None], (size, *value.shape)), axis,...]
    all_to_all x1, starting transfers between devices: 9.99 us -> 5.15 us  [shards(): lax.all_to_all(produced, 'ep', split_axis=1, concat_axis=0, tiled=True)]
    reduce_sum x1, other arithmetic: 3.23 us -> 0.9 us  [shards(): squares = jnp.sum(jnp.square(portion.astype(jnp.float32)), axis=2)]
    all_gather x1, waiting for transfers between devices: 0.02 us -> 2.28 us  [shards(): lax.all_gather(pooled, 'tp', axis=1, tiled=True)]
    all_to_all x1, waiting for transfers between devices: 9.79 us -> 7.54 us  [shards(): lax.all_to_all(produced, 'ep', split_axis=1, concat_axis=0, tiled=True)]
  transfers between devices with their start and end apart: 5 -> 19, of which waited for: 3 -> 17; matrix products, arithmetic and copies ran while one was open for 9% -> 8% of each run, Pallas kernels for 0% -> 0%
where the time goes in v1:
time: 196 us
  waiting for transfers between devices  72.7 us (37%)
  starting transfers between devices  56.5 us (29%)
  blocking collectives  25.8 us (13%)
  between operations  14.8 us (8%)
  local copies, waits for them, and re-layouts  12.6 us (6%)
  other arithmetic  7.06 us (4%)
  matrix products  6.56 us (3%)
    all_to_all x1, waiting for transfers between devices, copy_for_each(): lax.all_to_all(jnp.broadcast_to(value[None], (size, *value.shape)), axis,...  52.7 us
    ppermute x8, starting transfers between devices, extend_heaps(): block_now = lax.ppermute(block_now, 'tp', steps_seen)  25.9 us
    all_to_all x1, blocking collectives, shards(): lax.all_to_all(outgoing, 'ep', split_axis=0, concat_axis=1, tiled=True)  25.8 us
    all_to_all x1, starting transfers between devices, copy_for_each(): lax.all_to_all(jnp.broadcast_to(value[None], (size, *value.shape)), axis,...  14.1 us
    ppermute x7, starting transfers between devices, extend_heaps(): built = lax.ppermute(built, 'tp', gallery)  9.03 us
    all_to_all x1, waiting for transfers between devices, shards(): lax.all_to_all(produced, 'ep', split_axis=1, concat_axis=0, tiled=True)  7.54 us
    ppermute x8, waiting for transfers between devices, extend_heaps(): block_now = lax.ppermute(block_now, 'tp', steps_seen)  6.49 us
    all_to_all x1, starting transfers between devices, shards(): lax.all_to_all(produced, 'ep', split_axis=1, concat_axis=0, tiled=True)  5.15 us
  transfers between devices with their start and end apart: 19, of which 17 were waited for; matrix products, arithmetic and copies ran while one was open for 8% of the time, Pallas kernels for 0%

profile of v1, /device:TPU:24, one launch (start us, length us, event | category | flops | bytes accessed | tf_op | source)
XLA Modules:
  0.0 195.9 jit_solution(11184812887582910)
XLA Ops:
  7.2 0.9 copy.27
  8.1 0.1 eq.45
  8.2 0.1 eq.41
  8.3 0.7 broadcast_multiply_fusion
  9.0 0.6 reduce-window.6
  9.6 0.2 slice_reduce_fusion
  10.0 0.1 mul.362
  10.1 0.1 reshape.270
  10.4 1.4 scatter_custom_fusion
  11.8 0.8 concatenate.7
  12.6 1.9 gather_fusion
  14.6 25.8 %all_to_all.26 = bf16[32,16,256]{2,1,0:T(8,128)(2,1)S(1)} all-to-all(bf16[32,16,256]{2,1,0:T(8,128)(2,1)S(1)} %bitcast.70), channel_id=1, replica_groups=mesh['ep'=32,'tp'=16] {'ep'}, dimensions={0} | all-to-all | bytes 524288 | tf_op jit(solution)/shard_map/all_to_all | solution.py:124
  40.4 0.7 slice.58
  41.1 2.1 %collective-permute-start = (bf16[15,128]{1,0:T(8,128)(2,1)S(1)}, bf16[15,128]{1,0:T(8,128)(2,1)S(1)}, u32[]{:S(2)}, u32[]{:S(2)}) collective-permute-start(bf16[15,128]{1,0:T(8,128)(2,1)S(1)} %slice.58), channel_id=1, source_target_pairs={{0,16},{16,32},{32,48},{48,64},{64,80},{80,96},{96,112},{112,128},... | collective-permute-start | bytes 11528 | tf_op jit(solution)/shard_map/ppermute | solution.py:15
  43.2 1.5 collective-permute-start.2
  44.7 1.5 collective-permute-done.1
  46.2 0.4 collective-permute-start.3
  46.6 1.9 collective-permute-done.2
  48.6 2.2 %collective-permute-start.4 = (bf16[1,512,256]{2,1,0:T(8,128)(2,1)S(1)}, bf16[1,512,256]{2,1,0:T(8,128)(2,1)S(1)}, u32[]{:S(2)}, u32[]{:S(2)}) collective-permute-start(bf16[1,512,256]{2,1,0:T(8,128)(2,1)S(1)} %collective-permute-done.2), channel_id=1, source_target_pairs={{0,15},{1,0},{2,1},{3,2},{4,3},{5,4},{6,5},{7,6},{8,7},{9,8},{10,9... | collective-permute-start | bytes 786440 | tf_op jit(solution)/shard_map/ppermute | solution.py:95
  50.8 1.2 collective-permute-done.3
  52.0 1.6 collective-permute-start.5
  53.6 1.0 collective-permute-done.4
  54.7 2.2 %collective-permute-start.6 = (bf16[1,512,256]{2,1,0:T(8,128)(2,1)S(1)}, bf16[1,512,256]{2,1,0:T(8,128)(2,1)S(1)}, u32[]{:S(2)}, u32[]{:S(2)}) collective-permute-start(bf16[1,512,256]{2,1,0:T(8,128)(2,1)S(1)} %collective-permute-done.4), channel_id=1, source_target_pairs={{0,15},{1,0},{2,1},{3,2},{4,3},{5,4},{6,5},{7,6},{8,7},{9,8},{10,9... | collective-permute-start | bytes 786440 | tf_op jit(solution)/shard_map/ppermute | solution.py:95
  57.2 0.6 collective-permute-done.5
  57.8 2.8 %collective-permute-start.7 = (bf16[1,512,256]{2,1,0:T(8,128)(2,1)S(1)}, bf16[1,512,256]{2,1,0:T(8,128)(2,1)S(1)}, u32[]{:S(2)}, u32[]{:S(2)}) collective-permute-start(bf16[1,512,256]{2,1,0:T(8,128)(2,1)S(1)} %collective-permute-done.5), channel_id=1, source_target_pairs={{0,1},{1,2},{2,3},{3,4},{4,5},{5,6},{6,7},{7,8},{8,9},{9,10},{10,1... | collective-permute-start | bytes 786440 | tf_op jit(solution)/shard_map/ppermute | solution.py:90
  60.6 0.5 broadcast_in_dim.167
  61.2 1.7 collective-permute-start.8
  63.0 0.6 collective-permute-done.7
  63.6 4.1 %collective-permute-start.9 = (bf16[1,512,256]{2,1,0:T(8,128)(2,1)S(1)}, bf16[1,512,256]{2,1,0:T(8,128)(2,1)S(1)}, u32[]{:S(2)}, u32[]{:S(2)}) collective-permute-start(bf16[1,512,256]{2,1,0:T(8,128)(2,1)S(1)} %collective-permute-done.7), channel_id=1, source_target_pairs={{0,1},{1,2},{2,3},{3,4},{4,5},{5,6},{6,7},{7,8},{8,9},{9,10},{10,1... | collective-permute-start | bytes 786440 | tf_op jit(solution)/shard_map/ppermute | solution.py:90
  67.7 0.2 collective-permute-done.8
  67.9 1.2 collective-permute-start.10
  69.1 0.3 collective-permute-done.9
  69.4 5.3 %collective-permute-start.11 = (bf16[1,512,256]{2,1,0:T(8,128)(2,1)S(1)}, bf16[1,512,256]{2,1,0:T(8,128)(2,1)S(1)}, u32[]{:S(2)}, u32[]{:S(2)}) collective-permute-start(bf16[1,512,256]{2,1,0:T(8,128)(2,1)S(1)} %collective-permute-done.9), channel_id=1, source_target_pairs={{0,1},{1,2},{2,3},{3,4},{4,5},{5,6},{6,7},{7,8},{8,9},{9,10},{10,1... | collective-permute-start | bytes 786440 | tf_op jit(solution)/shard_map/ppermute | solution.py:90
  74.7 0.2 collective-permute-done.10
  74.9 0.2 collective-permute-start.12
  75.2 0.6 collective-permute-done.11
  75.8 5.8 %collective-permute-start.13 = (bf16[1,512,256]{2,1,0:T(8,128)(2,1)S(1)}, bf16[1,512,256]{2,1,0:T(8,128)(2,1)S(1)}, u32[]{:S(2)}, u32[]{:S(2)}) collective-permute-start(bf16[1,512,256]{2,1,0:T(8,128)(2,1)S(1)} %collective-permute-done.11), channel_id=1, source_target_pairs={{0,1},{1,2},{2,3},{3,4},{4,5},{5,6},{6,7},{7,8},{8,9},{9,10},{10,1... | collective-permute-start | bytes 786440 | tf_op jit(solution)/shard_map/ppermute | solution.py:90
  81.7 0.2 collective-permute-done.12
  81.9 0.9 collective-permute-done.13
  82.8 5.8 %collective-permute-start.15 = (bf16[1,512,256]{2,1,0:T(8,128)(2,1)S(1)}, bf16[1,512,256]{2,1,0:T(8,128)(2,1)S(1)}, u32[]{:S(2)}, u32[]{:S(2)}) collective-permute-start(bf16[1,512,256]{2,1,0:T(8,128)(2,1)S(1)} %collective-permute-done.13), channel_id=1, source_target_pairs={{0,1},{1,2},{2,3},{3,4},{4,5},{5,6},{6,7},{7,8},{8,9},{9,10},{10,1... | collective-permute-start | bytes 786440 | tf_op jit(solution)/shard_map/ppermute | solution.py:90
  88.7 0.2 collective-permute-done.14
  88.9 0.9 collective-permute-done.15
  89.8 0.9 fusion.1
  90.8 1.3 fusion.8
  92.1 1.3 multiply_convert_fusion
  93.3 0.1 copy.30
  93.5 1.5 broadcast_in_dim.171
  95.0 14.1 %all-to-all-start.1 = ((bf16[16,1,512,128]{2,3,1,0:T(8,128)(2,1)}), bf16[16,1,512,128]{2,3,1,0:T(8,128)(2,1)S(1)}, u32[]{:S(2)}, u32[]{:S(2)}) async-start(bf16[16,1,512,128]{2,3,1,0:T(8,128)(2,1)} %broadcast_in_dim.171), calls=%async_computation.1 | async-start | bytes 4194304 | tf_op jit(solution)/shard_map/all_to_all | solution.py:26
  109.1 0.2 all-gather.2.cloned.1.call-start
  109.4 1.2 fusion.34
  110.7 52.7 %all-to-all-done.1 = bf16[16,1,512,128]{2,3,1,0:T(8,128)(2,1)S(1)} async-done(((bf16[16,1,512,128]{2,3,1,0:T(8,128)(2,1)}), bf16[16,1,512,128]{2,3,1,0:T(8,128)(2,1)S(1)}, u32[]{:S(2)}, u32[]{:S(2)}) %all-to-all-start.1) | async-done | bytes 2097184 | tf_op jit(solution)/shard_map/all_to_all | solution.py:26
  163.4 0.8 fusion.7
  164.1 0.4 copy.40
  164.6 0.5 broadcast.1960
  165.1 2.2 %reduce.3 = bf16[512,256]{1,0:T(8,128)(2,1)S(1)} reduce(bf16[512,1,256]{2,1,0:T(2,128)(2,1)S(1)} %bitcast.66, bf16[]{:T(256)} %broadcast.1960), dimensions={1}, to_apply=%bitcast.61.reduce_sub_computation | reduce | bytes 524290
  167.3 0.8 reshape.278
  168.1 5.2 %all-to-all-start.2 = ((bf16[32,2,2048]{2,1,0:T(2,128)(2,1)}), bf16[32,2,2048]{2,1,0:T(2,128)(2,1)S(1)}, u32[]{:S(2)}, u32[]{:S(2)}) async-start(bf16[32,2,2048]{2,1,0:T(2,128)(2,1)} %reshape.278), calls=%async_computation.2 | async-start | bytes 524288 | tf_op jit(solution)/shard_map/all_to_all | solution.py:138
  173.4 2.3 %all-gather.2.cloned.1.call-done = bf16[512,2048]{1,0:T(8,128)(2,1)} async-done(((bf16[512,128]{1,0:T(8,128)(2,1)}), bf16[512,2048]{1,0:T(8,128)(2,1)}) %all-gather.2.cloned.1.call-update) | async-done | bytes 2097168 | tf_op jit(solution)/shard_map/all_gather | solution.py:109
  175.6 3.3 %convolution_convert_fusion.1 = bf16[512,256]{1,0:T(8,128)(2,1)} fusion(bf16[512,2048]{1,0:T(8,128)(2,1)} %all-gather.2.cloned.1.call-done, bf16[2048,256]{1,0:T(8,128)(2,1)} %param.10), kind=kOutput, calls=%fused_computation.11 | convolution fusion | flops 537001984 | bytes 3407872 | tf_op jit(solution)/shard_map/dot_general | solution.py:108
  178.9 7.5 %all-to-all-done.2 = bf16[32,2,2048]{2,1,0:T(2,128)(2,1)S(1)} async-done(((bf16[32,2,2048]{2,1,0:T(2,128)(2,1)}), bf16[32,2,2048]{2,1,0:T(2,128)(2,1)S(1)}, u32[]{:S(2)}, u32[]{:S(2)}) %all-to-all-start.2) | async-done | bytes 262176 | tf_op jit(solution)/shard_map/all_to_all | solution.py:138
  186.4 0.3 reshape.279
  186.8 1.2 gather_fusion.1
  187.9 0.1 reshape.249
  188.1 1.0 multiply_reduce_fusion
  (59 shorter events, 1.2 us)
Async XLA Ops:
  7.2 156.2 %copy-start = (bf16[1,2048,256]{2,1,0:T(8,128)(2,1)S(1)}, bf16[1,2048,256]{2,1,0:T(8,128)(2,1)}, u32[]{:S(2)}) copy-start(bf16[1,2048,256]{2,1,0:T(8,128)(2,1)} %param.17) | copy-start | bytes 3145732
  40.4 5.8 %collective-permute-start.1 = (bf16[1,512,256]{2,1,0:T(8,128)(2,1)S(1)}, bf16[1,512,256]{2,1,0:T(8,128)(2,1)S(1)}, u32[]{:S(2)}, u32[]{:S(2)}) collective-permute-start(bf16[1,512,256]{2,1,0:T(8,128)(2,1)S(1)} %bitcast.67), channel_id=1, source_target_pairs={{0,1},{1,2},{2,3},{3,4},{4,5},{5,6},{6,7},{7,8},{8,9},{9,10},{10,1... | collective-permute-start | bytes 786440 | tf_op jit(solution)/shard_map/ppermute | solution.py:90
  41.1 68.3 %collective-permute-start = (bf16[15,128]{1,0:T(8,128)(2,1)S(1)}, bf16[15,128]{1,0:T(8,128)(2,1)S(1)}, u32[]{:S(2)}, u32[]{:S(2)}) collective-permute-start(bf16[15,128]{1,0:T(8,128)(2,1)S(1)} %slice.58), channel_id=1, source_target_pairs={{0,16},{16,32},{32,48},{48,64},{64,80},{80,96},{96,112},{112,128},... | collective-permute-start | bytes 11528 | tf_op jit(solution)/shard_map/ppermute | solution.py:15
  43.2 5.4 %collective-permute-start.2 = (bf16[1,512,256]{2,1,0:T(8,128)(2,1)S(1)}, bf16[1,512,256]{2,1,0:T(8,128)(2,1)S(1)}, u32[]{:S(2)}, u32[]{:S(2)}) collective-permute-start(bf16[1,512,256]{2,1,0:T(8,128)(2,1)S(1)} %bitcast.68), channel_id=1, source_target_pairs={{0,15},{1,0},{2,1},{3,2},{4,3},{5,4},{6,5},{7,6},{8,7},{9,8},{10,9... | collective-permute-start | bytes 786440 | tf_op jit(solution)/shard_map/ppermute | solution.py:95
  46.2 5.8 %collective-permute-start.3 = (bf16[1,512,256]{2,1,0:T(8,128)(2,1)S(1)}, bf16[1,512,256]{2,1,0:T(8,128)(2,1)S(1)}, u32[]{:S(2)}, u32[]{:S(2)}) collective-permute-start(bf16[1,512,256]{2,1,0:T(8,128)(2,1)S(1)} %collective-permute-done.1), channel_id=1, source_target_pairs={{0,1},{1,2},{2,3},{3,4},{4,5},{5,6},{6,7},{7,8},{8,9},{9,10},{10,1... | collective-permute-start | bytes 786440 | tf_op jit(solution)/shard_map/ppermute | solution.py:90
  48.6 6.1 %collective-permute-start.4 = (bf16[1,512,256]{2,1,0:T(8,128)(2,1)S(1)}, bf16[1,512,256]{2,1,0:T(8,128)(2,1)S(1)}, u32[]{:S(2)}, u32[]{:S(2)}) collective-permute-start(bf16[1,512,256]{2,1,0:T(8,128)(2,1)S(1)} %collective-permute-done.2), channel_id=1, source_target_pairs={{0,15},{1,0},{2,1},{3,2},{4,3},{5,4},{6,5},{7,6},{8,7},{9,8},{10,9... | collective-permute-start | bytes 786440 | tf_op jit(solution)/shard_map/ppermute | solution.py:95
  52.0 5.8 %collective-permute-start.5 = (bf16[1,512,256]{2,1,0:T(8,128)(2,1)S(1)}, bf16[1,512,256]{2,1,0:T(8,128)(2,1)S(1)}, u32[]{:S(2)}, u32[]{:S(2)}) collective-permute-start(bf16[1,512,256]{2,1,0:T(8,128)(2,1)S(1)} %collective-permute-done.3), channel_id=1, source_target_pairs={{0,1},{1,2},{2,3},{3,4},{4,5},{5,6},{6,7},{7,8},{8,9},{9,10},{10,1... | collective-permute-start | bytes 786440 | tf_op jit(solution)/shard_map/ppermute | solution.py:90
  54.7 6.5 %collective-permute-start.6 = (bf16[1,512,256]{2,1,0:T(8,128)(2,1)S(1)}, bf16[1,512,256]{2,1,0:T(8,128)(2,1)S(1)}, u32[]{:S(2)}, u32[]{:S(2)}) collective-permute-start(bf16[1,512,256]{2,1,0:T(8,128)(2,1)S(1)} %collective-permute-done.4), channel_id=1, source_target_pairs={{0,15},{1,0},{2,1},{3,2},{4,3},{5,4},{6,5},{7,6},{8,7},{9,8},{10,9... | collective-permute-start | bytes 786440 | tf_op jit(solution)/shard_map/ppermute | solution.py:95
  57.8 5.8 %collective-permute-start.7 = (bf16[1,512,256]{2,1,0:T(8,128)(2,1)S(1)}, bf16[1,512,256]{2,1,0:T(8,128)(2,1)S(1)}, u32[]{:S(2)}, u32[]{:S(2)}) collective-permute-start(bf16[1,512,256]{2,1,0:T(8,128)(2,1)S(1)} %collective-permute-done.5), channel_id=1, source_target_pairs={{0,1},{1,2},{2,3},{3,4},{4,5},{5,6},{6,7},{7,8},{8,9},{9,10},{10,1... | collective-permute-start | bytes 786440 | tf_op jit(solution)/shard_map/ppermute | solution.py:90
  61.2 6.7 %collective-permute-start.8 = (bf16[1,512,256]{2,1,0:T(8,128)(2,1)S(1)}, bf16[1,512,256]{2,1,0:T(8,128)(2,1)S(1)}, u32[]{:S(2)}, u32[]{:S(2)}) collective-permute-start(bf16[1,512,256]{2,1,0:T(8,128)(2,1)S(1)} %collective-permute-done.6), channel_id=1, source_target_pairs={{0,15},{1,0},{2,1},{3,2},{4,3},{5,4},{6,5},{7,6},{8,7},{9,8},{10,9... | collective-permute-start | bytes 786440 | tf_op jit(solution)/shard_map/ppermute | solution.py:95
  63.6 5.8 %collective-permute-start.9 = (bf16[1,512,256]{2,1,0:T(8,128)(2,1)S(1)}, bf16[1,512,256]{2,1,0:T(8,128)(2,1)S(1)}, u32[]{:S(2)}, u32[]{:S(2)}) collective-permute-start(bf16[1,512,256]{2,1,0:T(8,128)(2,1)S(1)} %collective-permute-done.7), channel_id=1, source_target_pairs={{0,1},{1,2},{2,3},{3,4},{4,5},{5,6},{6,7},{7,8},{8,9},{9,10},{10,1... | collective-permute-start | bytes 786440 | tf_op jit(solution)/shard_map/ppermute | solution.py:90
  67.9 7.0 %collective-permute-start.10 = (bf16[1,512,256]{2,1,0:T(8,128)(2,1)S(1)}, bf16[1,512,256]{2,1,0:T(8,128)(2,1)S(1)}, u32[]{:S(2)}, u32[]{:S(2)}) collective-permute-start(bf16[1,512,256]{2,1,0:T(8,128)(2,1)S(1)} %collective-permute-done.8), channel_id=1, source_target_pairs={{0,15},{1,0},{2,1},{3,2},{4,3},{5,4},{6,5},{7,6},{8,7},{9,8},{10,9... | collective-permute-start | bytes 786440 | tf_op jit(solution)/shard_map/ppermute | solution.py:95
  69.4 6.4 %collective-permute-start.11 = (bf16[1,512,256]{2,1,0:T(8,128)(2,1)S(1)}, bf16[1,512,256]{2,1,0:T(8,128)(2,1)S(1)}, u32[]{:S(2)}, u32[]{:S(2)}) collective-permute-start(bf16[1,512,256]{2,1,0:T(8,128)(2,1)S(1)} %collective-permute-done.9), channel_id=1, source_target_pairs={{0,1},{1,2},{2,3},{3,4},{4,5},{5,6},{6,7},{7,8},{8,9},{9,10},{10,1... | collective-permute-start | bytes 786440 | tf_op jit(solution)/shard_map/ppermute | solution.py:90
  74.7 16.1 %copy-start.3 = (bf16[1,4096,128]{2,1,0:T(8,128)(2,1)S(1)}, bf16[1,4096,128]{2,1,0:T(8,128)(2,1)}, u32[]{:S(2)}) copy-start(bf16[1,4096,128]{2,1,0:T(8,128)(2,1)} %param.15) | copy-start | bytes 3145732
  74.7 16.1 %copy-start.5 = (f32[4096]{0:T(1024)S(1)}, f32[4096]{0:T(1024)}, u32[]{:S(2)}) copy-start(f32[4096]{0:T(1024)} %param.14) | copy-start | bytes 49156
  74.9 7.0 %collective-permute-start.12 = (bf16[1,512,256]{2,1,0:T(8,128)(2,1)S(1)}, bf16[1,512,256]{2,1,0:T(8,128)(2,1)S(1)}, u32[]{:S(2)}, u32[]{:S(2)}) collective-permute-start(bf16[1,512,256]{2,1,0:T(8,128)(2,1)S(1)} %collective-permute-done.10), channel_id=1, source_target_pairs={{0,15},{1,0},{2,1},{3,2},{4,3},{5,4},{6,5},{7,6},{8,7},{9,8},{10,9... | collective-permute-start | bytes 786440 | tf_op jit(solution)/shard_map/ppermute | solution.py:95
  75.8 7.0 %collective-permute-start.13 = (bf16[1,512,256]{2,1,0:T(8,128)(2,1)S(1)}, bf16[1,512,256]{2,1,0:T(8,128)(2,1)S(1)}, u32[]{:S(2)}, u32[]{:S(2)}) collective-permute-start(bf16[1,512,256]{2,1,0:T(8,128)(2,1)S(1)} %collective-permute-done.11), channel_id=1, source_target_pairs={{0,1},{1,2},{2,3},{3,4},{4,5},{5,6},{6,7},{7,8},{8,9},{9,10},{10,1... | collective-permute-start | bytes 786440 | tf_op jit(solution)/shard_map/ppermute | solution.py:90
  81.9 7.0 %collective-permute-start.14 = (bf16[1,512,256]{2,1,0:T(8,128)(2,1)S(1)}, bf16[1,512,256]{2,1,0:T(8,128)(2,1)S(1)}, u32[]{:S(2)}, u32[]{:S(2)}) collective-permute-start(bf16[1,512,256]{2,1,0:T(8,128)(2,1)S(1)} %collective-permute-done.12), channel_id=1, source_target_pairs={{0,15},{1,0},{2,1},{3,2},{4,3},{5,4},{6,5},{7,6},{8,7},{9,8},{10,9... | collective-permute-start | bytes 786440 | tf_op jit(solution)/shard_map/ppermute | solution.py:95
  82.8 7.0 %collective-permute-start.15 = (bf16[1,512,256]{2,1,0:T(8,128)(2,1)S(1)}, bf16[1,512,256]{2,1,0:T(8,128)(2,1)S(1)}, u32[]{:S(2)}, u32[]{:S(2)}) collective-permute-start(bf16[1,512,256]{2,1,0:T(8,128)(2,1)S(1)} %collective-permute-done.13), channel_id=1, source_target_pairs={{0,1},{1,2},{2,3},{3,4},{4,5},{5,6},{6,7},{7,8},{8,9},{9,10},{10,1... | collective-permute-start | bytes 786440 | tf_op jit(solution)/shard_map/ppermute | solution.py:90
  90.7 1.3 copy-start.4
  93.3 16.0 %copy-start.1 = (bf16[512,128]{1,0:T(8,128)(2,1)S(1)}, bf16[512,128]{1,0:T(8,128)(2,1)}, u32[]{:S(2)}) copy-start(bf16[512,128]{1,0:T(8,128)(2,1)} %param.9) | copy-start | bytes 393220
  95.0 15.7 %copy-start.2 = (f32[128,2]{0,1:T(2,128)S(1)}, f32[128,2]{0,1:T(2,128)}, u32[]{:S(2)}) copy-start(f32[128,2]{0,1:T(2,128)} %param.13) | copy-start | bytes 3076
  95.0 68.4 %all-to-all-start.1 = ((bf16[16,1,512,128]{2,3,1,0:T(8,128)(2,1)}), bf16[16,1,512,128]{2,3,1,0:T(8,128)(2,1)S(1)}, u32[]{:S(2)}, u32[]{:S(2)}) async-start(bf16[16,1,512,128]{2,3,1,0:T(8,128)(2,1)} %broadcast_in_dim.171), calls=%async_computation.1 | async-start | bytes 4194304 | tf_op jit(solution)/shard_map/all_to_all | solution.py:26
  109.1 66.5 %all-gather.2.cloned.1.call-start = ((), (), s32[]{:S(2)}) async-start(), calls=%async_computation.3 | async-start | bytes 2228224 | tf_op jit(solution)/shard_map/all_gather | solution.py:109
  168.1 18.4 %all-to-all-start.2 = ((bf16[32,2,2048]{2,1,0:T(2,128)(2,1)}), bf16[32,2,2048]{2,1,0:T(2,128)(2,1)S(1)}, u32[]{:S(2)}, u32[]{:S(2)}) async-start(bf16[32,2,2048]{2,1,0:T(2,128)(2,1)} %reshape.278), calls=%async_computation.2 | async-start | bytes 524288 | tf_op jit(solution)/shard_map/all_to_all | solution.py:138
Sparse Core Ops, SparseCore 0:
  112.5 63.0 all-gather.1
